TPU v7x, 512 devices: a 8x2x16 block of a 8x8x16 slice. The times are simulated.
512 devices in a mesh: grp: 2 (over y), dp: 8 (over x), kv: 16 (over z), tp: 2 (over core).
Axes of the slice: x: 8, y: 2, z: 16, core: 2. Of those that a mesh axis runs over, the one named last changes fastest.
The devices are a block of a 8x8x16 slice.
Arguments:
- tokens: bfloat16 [512, 2048], P(('grp', 'dp'), ('kv', 'tp')), parts along dimension 0, may hold values from -24 to 24
- memory: float32 [512, 12, 16384], P(('grp', 'dp', 'kv', 'tp')), parts along dimension 0, may hold values from -3 to 3
- mix_gain: float32 [2048], replicated, may hold values from 0.1 to 1.9
- w_query: bfloat16 [2048, 1536], P(None, ('kv', 'tp')), may hold values from -0.125 to 0.125
- w_key: bfloat16 [2048, 1536], P(None, ('kv', 'tp')), may hold values from -0.125 to 0.125
- w_value: bfloat16 [2048, 1536], P(None, ('kv', 'tp')), may hold values from -0.125 to 0.125
- w_gate: bfloat16 [2048, 1536], P(None, ('kv', 'tp')), may hold values from -0.125 to 0.125
- w_beta: bfloat16 [2048, 12], replicated, may hold values from -0.125 to 0.125
- w_decay: bfloat16 [2048, 12], replicated, may hold values from -0.125 to 0.125
- decay_rate: float32 [12], replicated, may hold values from 0.1 to 3
- decay_bias: float32 [12], replicated, may hold values from -2 to 1
- head_gain: float32 [128], replicated, may hold values from 0.1 to 1.9
- w_out: bfloat16 [1536, 2048], P(None, ('kv', 'tp')), may hold values from -0.15625 to 0.15625
- ffn_gain: float32 [2048], replicated, may hold values from 0.1 to 1.9
- w_up: bfloat16 [2048, 8192], P(None, ('kv', 'tp')), may hold values from -0.125 to 0.125
- w_down: bfloat16 [8192, 2048], P(('kv', 'tp')), may hold values from -0.125 to 0.125
Outputs:
- layer_out: bfloat16 [512, 2048], P(('grp', 'dp'), ('kv', 'tp')), parts along dimension 0
- new_memory: float32 [512, 12, 16384], P(('grp', 'dp', 'kv', 'tp')), parts along dimension 0
There are 2 independent parts, one for each index of `grp`. A program takes and returns all parts, laid end to end along the dimension named above; an argument that names none is the same for every part. Nothing has to cross between parts.
All inputs are finite; a program needn't handle non-finite values.
Results may differ from a plain program's by a relative error of at most 0.02.
Values may be sent and summed in bfloat16 or wider, within the bound.
A program may use at most 64 MiB of HBM per device.

v0:
```python
import jax
import jax.numpy as jnp
from jax import lax
from jax.sharding import PartitionSpec as P

epsilon = 1e-06


def in_order(pieces, dim):
    pieces = jnp.moveaxis(pieces, 0, dim)
    dims = pieces.shape
    return pieces.reshape(*dims[:dim], dims[dim] * dims[dim + 1], *dims[dim + 2 :])


def from_everyone(value, axis):
    size = lax.axis_size(axis)
    return lax.all_to_all(
        jnp.broadcast_to(value[None], (size, *value.shape)), axis, 0, 0, tiled=True
    )


def gathered_copies(value, axis, dim):
    return in_order(from_everyone(value, axis), dim)


def shortened(value):
    return jax.tree.map(lambda a: a.astype(jnp.bfloat16) if a.dtype == jnp.float32 else a, value)


def cut_along(value, dim, size):
    before, after = (value.shape[:dim], value.shape[dim + 1 :])
    return jnp.moveaxis(value.reshape(*before, size, -1, *after), dim, 0)


def sum_at_owner(value, axis, dim):
    size = lax.axis_size(axis)
    pieces = lax.all_to_all(cut_along(value, dim, size), axis, 0, 0, tiled=True)
    return jnp.sum(pieces.astype(jnp.float32), axis=0)


def delta_step(queries, keys_in, values, gates, strength, log_decay, memory, head_gain):
    count = queries.shape[0]
    heads = strength.shape[1]
    size = head_gain.shape[0]
    query_wide = queries.astype(jnp.float32).reshape(count, heads, size)
    key_wide = keys_in.astype(jnp.float32).reshape(count, heads, size)
    value_wide = values.astype(jnp.float32).reshape(count, heads, size)
    gate_wide = gates.astype(jnp.float32).reshape(count, heads, size)
    unit_key = key_wide * lax.rsqrt(jnp.sum(key_wide * key_wide, axis=-1, keepdims=True) + epsilon)
    matrix = memory.reshape(count, heads, size, size)
    recall = jnp.einsum("bhk,bhkv->bhv", unit_key, matrix)
    retain = jnp.exp(log_decay)[:, :, None, None]
    scaled = strength[:, :, None]
    erased = matrix - jnp.einsum("bhk,bhv->bhkv", unit_key, scaled * recall)
    written = jnp.einsum("bhk,bhv->bhkv", unit_key, scaled * value_wide)
    updated = retain * erased + written
    readout = jnp.einsum("bhk,bhkv->bhv", query_wide, updated)
    normed = readout * lax.rsqrt(jnp.mean(readout * readout, axis=-1, keepdims=True) + epsilon)
    normed = normed * head_gain * jax.nn.silu(gate_wide)
    return (
        updated.reshape(count, heads, size * size),
        normed.reshape(count, heads * size).astype(jnp.bfloat16),
    )


def per_device(
    tokens,
    memory,
    mix_gain,
    w_query,
    w_key,
    w_value,
    w_gate,
    w_beta,
    w_decay,
    decay_rate,
    decay_bias,
    head_gain,
    w_out,
    ffn_gain,
    w_up,
    w_down,
):
    rows = tokens.shape[0]
    columns = tokens.shape[1]
    owned = memory.shape[0]
    width = mix_gain.shape[0]
    lane = lax.axis_index(("kv", "tp"))
    own_start = lane * owned
    wide = tokens.astype(jnp.float32)
    head_weights = (w_query, w_key, w_value, w_gate)
    small_weights = (w_beta, w_decay)

    def fold_proj(carry, piece, start):
        mine = lax.dynamic_slice_in_dim(piece, own_start, owned, 0)
        large = tuple(
            (jnp.dot(piece, weight, preferred_element_type=jnp.float32) for weight in head_weights)
        )
        small = tuple(
            (jnp.dot(mine, weight, preferred_element_type=jnp.float32) for weight in small_weights)
        )
        return large + small

    def fold_up(total, piece, start):
        return jnp.dot(piece, w_up, preferred_element_type=jnp.float32)

    def with_squares(inner, gain, carry, piece, start):
        piece_wide = piece.astype(jnp.float32)
        lifted = (piece_wide * gain).astype(jnp.bfloat16)
        return (inner(carry[0], lifted, start), jnp.sum(piece_wide * piece_wide, axis=1))

    proj_init = tuple((jnp.zeros((rows, weight.shape[1]), jnp.float32) for weight in head_weights))
    proj_init = proj_init + tuple(
        (jnp.zeros((owned, weight.shape[1]), jnp.float32) for weight in small_weights)
    )
    row_zeros = jnp.zeros((rows,), jnp.float32)
    folded, total_in = with_squares(
        fold_proj,
        mix_gain,
        (proj_init, row_zeros),
        gathered_copies(tokens, ("kv", "tp"), 1),
        jnp.int32(0),
    )
    scale_in = lax.rsqrt(total_in / width + epsilon)
    sent = tuple(((total * scale_in[:, None]).astype(jnp.bfloat16) for total in folded[:4]))
    scale_own = lax.dynamic_slice_in_dim(scale_in, own_start, owned)[:, None]
    strength = jax.nn.sigmoid(folded[4] * scale_own)
    log_decay = -decay_rate * jax.nn.softplus(folded[5] * scale_own + decay_bias)
    queries, keys_in, values, gates = jax.tree.map(
        lambda part, own: part.astype(own.dtype),
        lax.all_to_all(shortened(sent), ("kv", "tp"), split_axis=0, concat_axis=1, tiled=True),
        sent,
    )
    updated, mixed = delta_step(
        queries, keys_in, values, gates, strength, log_decay, memory, head_gain
    )
    branch = jnp.dot(
        gathered_copies(mixed, ("kv", "tp"), 0), w_out, preferred_element_type=jnp.float32
    )
    middle = (wide + branch).astype(jnp.bfloat16)
    middle_wide = middle.astype(jnp.float32)
    up_init = jnp.zeros((rows, w_up.shape[1]), jnp.float32)
    raised, total_mid = with_squares(
        fold_up,
        ffn_gain,
        (up_init, row_zeros),
        gathered_copies(middle, ("kv", "tp"), 1),
        jnp.int32(0),
    )
    scale_mid = lax.rsqrt(total_mid / width + epsilon)[:, None]
    hidden = jnp.square(jax.nn.relu(raised * scale_mid)).astype(jnp.bfloat16)
    terms = jnp.dot(hidden, w_down, preferred_element_type=jnp.float32)
    blocks = terms.reshape(rows, lax.axis_size("kv"), lax.axis_size("tp"), columns)
    within = sum_at_owner(blocks.astype(jnp.bfloat16), "tp", 2)
    down = sum_at_owner(within.astype(jnp.bfloat16), "kv", 1).reshape(rows, columns)
    layer_out = (middle_wide + down).astype(jnp.bfloat16)
    return (layer_out, updated)


def solution(mesh):
    placed = (
        P(("grp", "dp"), ("kv", "tp")),
        P(("grp", "dp", "kv", "tp"), None, None),
        P(),
        P(None, ("kv", "tp")),
        P(None, ("kv", "tp")),
        P(None, ("kv", "tp")),
        P(None, ("kv", "tp")),
        P(),
        P(),
        P(),
        P(),
        P(),
        P(None, ("kv", "tp")),
        P(),
        P(None, ("kv", "tp")),
        P(("kv", "tp"), None),
    )
    return jax.shard_map(
        per_device,
        mesh=mesh,
        in_specs=placed,
        out_specs=(P(("grp", "dp"), ("kv", "tp")), P(("grp", "dp", "kv", "tp"), None, None)),
        check_vma=False,
    )
```

profile of v0, /device:TPU:65, one launch (start us, length us, event | category | flops | bytes accessed | tf_op | source)
XLA Modules:
  0.0 201.3 jit_solution(14850103766264147078)
XLA Ops:
  0.6 0.8 broadcast_in_dim.6
  1.5 0.8 reshape.301
  2.3 45.2 %all-to-all-start = ((bf16[32,2,1024]{2,1,0:T(2,128)(2,1)}), bf16[32,2,1024]{2,1,0:T(2,128)(2,1)S(1)}, u32[]{:S(2)}, u32[]{:S(2)}) async-start(bf16[32,2,1024]{2,1,0:T(2,128)(2,1)} %reshape.301), calls=%async_computation | async-start | bytes 262144 | tf_op jit(solution)/shard_map/all_to_all | solution.py:17
  47.5 15.9 %all-to-all-done = bf16[32,2,1024]{2,1,0:T(2,128)(2,1)S(1)} async-done(((bf16[32,2,1024]{2,1,0:T(2,128)(2,1)}), bf16[32,2,1024]{2,1,0:T(2,128)(2,1)S(1)}, u32[]{:S(2)}, u32[]{:S(2)}) %all-to-all-start) | async-done | bytes 131104 | tf_op jit(solution)/shard_map/all_to_all | solution.py:17
  64.4 0.6 dynamic_slice.7
  65.0 0.9 copy-done.12
  66.1 0.7 copy-done.13
  67.0 0.7 copy.34
  67.7 5.2 %all-to-all-start.2 = ((bf16[32,1,48]{2,1,0:T(2,128)(2,1)}), bf16[32,1,48]{2,1,0:T(2,128)(2,1)S(1)}, u32[]{:S(2)}, u32[]{:S(2)}) async-start(bf16[32,1,48]{2,1,0:T(2,128)(2,1)} %copy.34), calls=%async_computation.2 | async-start | bytes 32768 | tf_op jit(solution)/shard_map/all_to_all | solution.py:131
  72.9 0.8 fusion.16
  73.7 0.8 fusion.42
  74.7 0.6 copy.35
  75.3 9.4 %all-to-all-done.2 = bf16[32,1,48]{2,1,0:T(2,128)(2,1)S(1)} async-done(((bf16[32,1,48]{2,1,0:T(2,128)(2,1)}), bf16[32,1,48]{2,1,0:T(2,128)(2,1)S(1)}, u32[]{:S(2)}, u32[]{:S(2)}) %all-to-all-start.2) | async-done | bytes 3104 | tf_op jit(solution)/shard_map/all_to_all | solution.py:131
  84.7 4.5 %all-to-all-start.3 = ((bf16[32,1,48]{2,1,0:T(2,128)(2,1)}), bf16[32,1,48]{2,1,0:T(2,128)(2,1)S(1)}, u32[]{:S(2)}, u32[]{:S(2)}) async-start(bf16[32,1,48]{2,1,0:T(2,128)(2,1)} %copy.35), calls=%async_computation.3 | async-start | bytes 32768 | tf_op jit(solution)/shard_map/all_to_all | solution.py:131
  89.4 0.7 copy.36
  90.1 0.6 copy.33
  90.7 10.5 %all-to-all-done.3 = bf16[32,1,48]{2,1,0:T(2,128)(2,1)S(1)} async-done(((bf16[32,1,48]{2,1,0:T(2,128)(2,1)}), bf16[32,1,48]{2,1,0:T(2,128)(2,1)S(1)}, u32[]{:S(2)}, u32[]{:S(2)}) %all-to-all-start.3) | async-done | bytes 3104 | tf_op jit(solution)/shard_map/all_to_all | solution.py:131
  101.1 4.6 %all-to-all-start.1 = ((bf16[32,1,48]{2,1,0:T(2,128)(2,1)}), bf16[32,1,48]{2,1,0:T(2,128)(2,1)S(1)}, u32[]{:S(2)}, u32[]{:S(2)}) async-start(bf16[32,1,48]{2,1,0:T(2,128)(2,1)} %copy.33), calls=%async_computation.1 | async-start | bytes 32768 | tf_op jit(solution)/shard_map/all_to_all | solution.py:131
  106.3 11.4 %all-to-all-done.1 = bf16[32,1,48]{2,1,0:T(2,128)(2,1)S(1)} async-done(((bf16[32,1,48]{2,1,0:T(2,128)(2,1)}), bf16[32,1,48]{2,1,0:T(2,128)(2,1)S(1)}, u32[]{:S(2)}, u32[]{:S(2)}) %all-to-all-start.1) | async-done | bytes 3104 | tf_op jit(solution)/shard_map/all_to_all | solution.py:131
  117.6 4.6 %all-to-all-start.4 = ((bf16[32,1,48]{2,1,0:T(2,128)(2,1)}), bf16[32,1,48]{2,1,0:T(2,128)(2,1)S(1)}, u32[]{:S(2)}, u32[]{:S(2)}) async-start(bf16[32,1,48]{2,1,0:T(2,128)(2,1)} %copy.36), calls=%async_computation.4 | async-start | bytes 32768 | tf_op jit(solution)/shard_map/all_to_all | solution.py:131
  122.5 11.6 %all-to-all-done.4 = bf16[32,1,48]{2,1,0:T(2,128)(2,1)S(1)} async-done(((bf16[32,1,48]{2,1,0:T(2,128)(2,1)}), bf16[32,1,48]{2,1,0:T(2,128)(2,1)S(1)}, u32[]{:S(2)}, u32[]{:S(2)}) %all-to-all-start.4) | async-done | bytes 3104 | tf_op jit(solution)/shard_map/all_to_all | solution.py:131
  135.2 0.6 copy-done.11
  136.1 0.5 broadcast.117
  136.6 1.2 reduce.28
  137.8 18.5 %all_to_all.77 = bf16[32,2,768]{2,1,0:T(2,128)(2,1)S(1)} all-to-all(bf16[32,2,768]{2,1,0:T(2,128)(2,1)S(1)} %reshape.303), channel_id=1, replica_groups=mesh['grp'=2,'dp'=8,'kv'=16,'tp'=2] {'kv','tp'}, dimensions={0} | all-to-all | bytes 196608 | tf_op jit(solution)/shard_map/all_to_all | solution.py:17
  156.4 0.8 copy-done.4
  157.7 20.0 %all_to_all.78 = bf16[32,2,1024]{2,1,0:T(2,128)(2,1)S(1)} all-to-all(bf16[32,2,1024]{2,1,0:T(2,128)(2,1)S(1)} %reshape.305), channel_id=1, replica_groups=mesh['grp'=2,'dp'=8,'kv'=16,'tp'=2] {'kv','tp'}, dimensions={0} | all-to-all | bytes 262144 | tf_op jit(solution)/shard_map/all_to_all | solution.py:17
  178.7 0.7 copy-done.3
  179.4 0.7 convolution_convert_fusion
  180.7 5.0 %all_to_all.79 = bf16[2,2,16384]{2,1,0:T(2,128)(2,1)S(1)} all-to-all(bf16[2,2,16384]{2,1,0:T(2,128)(2,1)S(1)} %reshape.307), channel_id=1, replica_groups=mesh['grp'=2,'dp'=8,'kv'=16,'tp'=2] {'tp'}, dimensions={0} | all-to-all | bytes 262144 | tf_op jit(solution)/shard_map/all_to_all | solution.py:37
  186.1 14.3 %all_to_all.80 = bf16[16,2,1024]{2,1,0:T(2,128)(2,1)S(1)} all-to-all(bf16[16,2,1024]{2,1,0:T(2,128)(2,1)S(1)} %reshape.309), channel_id=1, replica_groups=mesh['grp'=2,'dp'=8,'kv'=16,'tp'=2] {'kv'}, dimensions={0} | all-to-all | bytes 131072 | tf_op jit(solution)/shard_map/all_to_all | solution.py:37
  200.7 0.6 add_convert_fusion
  (80 shorter events, 6.3 us)
Async XLA Ops:
  0.6 178.1 %copy-start = (bf16[256,2048]{1,0:T(8,128)(2,1)S(1)}, bf16[256,2048]{1,0:T(8,128)(2,1)}, u32[]{:S(2)}) copy-start(bf16[256,2048]{1,0:T(8,128)(2,1)} %param.31) | copy-start | bytes 3145732
  2.3 61.1 %all-to-all-start = ((bf16[32,2,1024]{2,1,0:T(2,128)(2,1)}), bf16[32,2,1024]{2,1,0:T(2,128)(2,1)S(1)}, u32[]{:S(2)}, u32[]{:S(2)}) async-start(bf16[32,2,1024]{2,1,0:T(2,128)(2,1)} %reshape.301), calls=%async_computation | async-start | bytes 262144 | tf_op jit(solution)/shard_map/all_to_all | solution.py:17
  64.2 0.8 copy-start.8
  65.0 0.9 copy-start.12
  65.9 0.9 copy-start.13
  65.9 6.9 %copy-start.16 = (bf16[2048,12]{0,1:T(8,128)(2,1)S(1)}, bf16[2048,12]{0,1:T(8,128)(2,1)}, u32[]{:S(2)}) copy-start(bf16[2048,12]{0,1:T(8,128)(2,1)} %param.23) | copy-start | bytes 147460
  65.9 7.7 %copy-start.5 = (bf16[2048,12]{0,1:T(8,128)(2,1)S(1)}, bf16[2048,12]{0,1:T(8,128)(2,1)}, u32[]{:S(2)}) copy-start(bf16[2048,12]{0,1:T(8,128)(2,1)} %param.24) | copy-start | bytes 147460
  65.9 7.7 %copy-start.9 = (f32[12]{0:T(128)S(1)}, f32[12]{0:T(128)}, u32[]{:S(2)}) copy-start(f32[12]{0:T(128)} %param.26) | copy-start | bytes 148
  65.9 7.7 %copy-start.10 = (f32[12]{0:T(128)S(1)}, f32[12]{0:T(128)}, u32[]{:S(2)}) copy-start(f32[12]{0:T(128)} %param.25) | copy-start | bytes 148
  66.0 8.5 %copy-start.14 = (bf16[2048,48]{0,1:T(8,128)(2,1)S(1)}, bf16[2048,48]{0,1:T(8,128)(2,1)}, u32[]{:S(2)}) copy-start(bf16[2048,48]{0,1:T(8,128)(2,1)} %param.21) | copy-start | bytes 589828
  66.0 23.3 %copy-start.15 = (bf16[2048,48]{0,1:T(8,128)(2,1)S(1)}, bf16[2048,48]{0,1:T(8,128)(2,1)}, u32[]{:S(2)}) copy-start(bf16[2048,48]{0,1:T(8,128)(2,1)} %param.19) | copy-start | bytes 589828
  66.9 67.4 %copy-start.1 = (f32[1,12,16384]{2,0,1:T(1,128)S(1)}, f32[1,12,16384]{2,0,1:T(1,128)}, u32[]{:S(2)}) copy-start(f32[1,12,16384]{2,0,1:T(1,128)} %param.17) | copy-start | bytes 2359300
  67.7 17.0 %all-to-all-start.2 = ((bf16[32,1,48]{2,1,0:T(2,128)(2,1)}), bf16[32,1,48]{2,1,0:T(2,128)(2,1)S(1)}, u32[]{:S(2)}, u32[]{:S(2)}) async-start(bf16[32,1,48]{2,1,0:T(2,128)(2,1)} %copy.34), calls=%async_computation.2 | async-start | bytes 32768 | tf_op jit(solution)/shard_map/all_to_all | solution.py:131
  84.7 16.4 %all-to-all-start.3 = ((bf16[32,1,48]{2,1,0:T(2,128)(2,1)}), bf16[32,1,48]{2,1,0:T(2,128)(2,1)S(1)}, u32[]{:S(2)}, u32[]{:S(2)}) async-start(bf16[32,1,48]{2,1,0:T(2,128)(2,1)} %copy.35), calls=%async_computation.3 | async-start | bytes 32768 | tf_op jit(solution)/shard_map/all_to_all | solution.py:131
  101.1 16.5 %all-to-all-start.1 = ((bf16[32,1,48]{2,1,0:T(2,128)(2,1)}), bf16[32,1,48]{2,1,0:T(2,128)(2,1)S(1)}, u32[]{:S(2)}, u32[]{:S(2)}) async-start(bf16[32,1,48]{2,1,0:T(2,128)(2,1)} %copy.33), calls=%async_computation.1 | async-start | bytes 32768 | tf_op jit(solution)/shard_map/all_to_all | solution.py:131
  117.6 16.4 %all-to-all-start.4 = ((bf16[32,1,48]{2,1,0:T(2,128)(2,1)}), bf16[32,1,48]{2,1,0:T(2,128)(2,1)S(1)}, u32[]{:S(2)}, u32[]{:S(2)}) async-start(bf16[32,1,48]{2,1,0:T(2,128)(2,1)} %copy.36), calls=%async_computation.4 | async-start | bytes 32768 | tf_op jit(solution)/shard_map/all_to_all | solution.py:131
  134.9 21.4 %copy-start.2 = (f32[12,128,128]{2,1,0:T(8,128)}, f32[12,128,128]{2,1,0:T(8,128)S(1)}, u32[]{:S(2)}) copy-start(f32[12,128,128]{2,1,0:T(8,128)S(1)} %multiply_add_fusion) | copy-start | bytes 2359300
  135.2 0.7 copy-start.11
  156.3 0.9 copy-start.4
  156.3 0.9 copy-start.6
  178.2 1.2 copy-start.3
  178.5 0.9 copy-start.7
where the time goes:
time: 202 us; the launch traced here: 201 us
  starting transfers between devices  64.1 us (32%)
  waiting for transfers between devices  58.8 us (29%)
  blocking collectives  57.8 us (29%)
  local copies, waits for them, and re-layouts  12.5 us (6%)
  matrix products  3.54 us (2%)
  other arithmetic  3.47 us (2%)
    all_to_all x1, starting transfers between devices, from_everyone(): lax.all_to_all(jnp.broadcast_to(value[None], (size, *value.shape)), axis,...  45.2 us
    all_to_all x4, waiting for transfers between devices, per_device(): lax.all_to_all(shortened(sent), ('kv', 'tp'), split_axis=0, concat_axis=1...  42.8 us
    all_to_all x2, blocking collectives, from_everyone(): lax.all_to_all(jnp.broadcast_to(value[None], (size, *value.shape)), axis,...  38.5 us
    all_to_all x2, blocking collectives, sum_at_owner(): pieces = lax.all_to_all(cut_along(value, dim, size), axis, 0, 0, tiled=True)  19.3 us
    all_to_all x4, starting transfers between devices, per_device(): lax.all_to_all(shortened(sent), ('kv', 'tp'), split_axis=0, concat_axis=1...  18.9 us
    all_to_all x1, waiting for transfers between devices, from_everyone(): lax.all_to_all(jnp.broadcast_to(value[None], (size, *value.shape)), axis,...  15.9 us
    unnamed x44, local copies, waits for them, and re-layouts  6.18 us
  transfers between devices with their start and end apart: 5, of which 5 were waited for; matrix products, arithmetic and copies ran while one was open for 2% of the time, Pallas kernels for 0%

commit v1 on v0

v1 whole, which is shorter than its diff:
```python
import functools
import jax
import jax.numpy as jnp
from jax import lax
from jax.experimental import pallas as pl
from jax.experimental.pallas import tpu as pltpu
from jax.sharding import PartitionSpec as P

epsilon = 1e-06
f32 = jnp.float32
bf16 = jnp.bfloat16
MESH = pl.DeviceIdType.MESH


def far_first(chips):
    return sorted(range(1, chips), key=lambda d: -min(d, chips - d))


def layer_kernel(
    tokens_hbm, memory_hbm, mix_gain_hbm, wq_hbm, wk_hbm, wv_hbm, wg_hbm, wbeta_hbm, wdecay_hbm,
    rate_hbm, bias_hbm, head_gain_hbm, wout_hbm, ffn_gain_hbm, wup_hbm, wdown_hbm,
    out_ref, new_memory_hbm,
    wproj, wsmall, wout, wup, wdown,
    state, state_out, tok, mix_gain, ffn_gain, rate, bias, head_gain,
    send1, buf1, send2, buf2, send3, buf3, send4, buf4, send5, buf5, midx,
    tokf, rawx, lift, scr_t, scr_a, scr_b, scr_c, scr_o,
    load_sem, wload_sem, wsend_sem, wrecv_sem, send_sem, recv_sem,
):
    chips = lax.axis_size("kv")
    cores = lax.axis_size("tp")
    z = lax.axis_index("kv")
    c = lax.axis_index("tp")
    other = 1 - c
    me = z * cores + c
    heads, size = 12, 128

    def chip_at(d):
        return lax.rem(z + d, chips)

    barrier = pltpu.get_barrier_semaphore()
    peers = [(d, k) for d in far_first(chips) for k in (0, 1)]
    for d, k in peers:
        pl.semaphore_signal(
            barrier, inc=1, device_id={"kv": chip_at(d), "tp": lax.rem(c + k, cores)},
            device_id_type=MESH,
        )
    pl.semaphore_signal(barrier, inc=1, device_id={"kv": z, "tp": other}, device_id_type=MESH)

    tok_copy = pltpu.make_async_copy(tokens_hbm, tok, load_sem.at[0])
    tok_copy.start()
    small = [
        pltpu.make_async_copy(src, dst, load_sem.at[1 + i])
        for i, (src, dst) in enumerate(
            (
                (mix_gain_hbm, mix_gain), (ffn_gain_hbm, ffn_gain), (rate_hbm, rate),
                (bias_hbm, bias), (head_gain_hbm, head_gain), (wbeta_hbm, wsmall.at[0]),
                (wdecay_hbm, wsmall.at[1]),
            )
        )
    ]
    for copy in small:
        copy.start()
    narrow, depth = wq_hbm.shape
    width = cores * narrow

    def rows_of(ref, start, count):
        return ref.at[pl.ds(pl.multiple_of(start + c * count, 16), count)]

    shared = [
        (wq_hbm, rows_of(wproj, 0, narrow)), (wk_hbm, rows_of(wproj, size, narrow)),
        (wv_hbm, rows_of(wproj, 2 * size, narrow)), (wg_hbm, rows_of(wproj, 3 * size, narrow)),
        (wout_hbm, rows_of(wout, 0, wout_hbm.shape[0])), (wup_hbm, wup.at[c]),
        (wdown_hbm, wdown.at[c]),
    ]
    own_weights = [
        pltpu.make_async_copy(src, dst, wload_sem.at[i])
        for i, (src, dst) in enumerate(shared)
    ]
    for copy in own_weights:
        copy.start()
    state_copy = pltpu.make_async_copy(memory_hbm, state, load_sem.at[8])
    state_copy.start()

    tok_copy.wait()
    tokf[:, 0 : tok.shape[1]] = tok[...].astype(f32)
    half_rows = chips // 2
    for k in range(2):
        part = tokf[pl.ds(k, chips, stride=2), :]
        cols = tok.shape[1]
        send1[k] = jnp.concatenate(
            [part[:half_rows, :cols], part[half_rows:, :cols]], axis=1
        ).astype(bf16)
    buf1[me] = send1[c]

    pl.semaphore_wait(barrier, len(peers) + 1)

    def send(src, dst, phase, d, core):
        pltpu.make_async_remote_copy(
            src_ref=src, dst_ref=dst, send_sem=send_sem.at[phase], recv_sem=recv_sem.at[phase],
            device_id={"kv": chip_at(d), "tp": core}, device_id_type=MESH,
        ).start()

    for d in far_first(chips):
        for k in range(2):
            core = lax.rem(c + k, cores)
            send(send1.at[core], buf1.at[me], 0, d, core)
    send(send1.at[other], buf1.at[me], 0, 0, other)

    swap = []
    for i, (src, dst) in enumerate(shared):
        copy = pltpu.make_async_remote_copy(
            src_ref=src, dst_ref=dst, send_sem=wsend_sem.at[i], recv_sem=wrecv_sem.at[i],
            device_id={"kv": z, "tp": other}, device_id_type=MESH,
        )
        copy.start()
        swap.append(copy)

    for copy in small:
        copy.wait()
    spare = size - width
    for x in range(4):
        if x < 2:
            rest = jnp.zeros((spare - heads, depth), bf16)
            rest = jnp.concatenate([wsmall[x].astype(f32), rest.astype(f32)], axis=0).astype(bf16)
        else:
            rest = jnp.zeros((spare, depth), bf16)
        wproj[x * size + width : (x + 1) * size, :] = rest
    for i in range(5):
        own_weights[i].wait()
        swap[i].wait_recv()

    def rows_dot(a, b):
        return lax.dot_general(a, b, (((1,), (1,)), ((), ())), preferred_element_type=f32)

    def arrived(buf, count, phase):
        pltpu.make_async_copy(
            buf.at[pl.ds(0, count)], buf.at[pl.ds(0, count)], recv_sem.at[phase]
        ).wait()

    def sent(buf, count, phase):
        pltpu.make_async_copy(
            buf.at[pl.ds(0, count)], buf.at[pl.ds(0, count)], send_sem.at[phase]
        ).wait()

    arrived(buf1, 2 * chips - 1, 0)
    squares = jnp.zeros((chips, size), f32)
    cols = size // 2
    for j in range(chips):
        even = buf1[2 * j].astype(f32)
        odd = buf1[2 * j + 1].astype(f32)
        top = jnp.concatenate([even[:, :cols], odd[:, :cols]], axis=1)
        low = jnp.concatenate([even[:, cols:], odd[:, cols:]], axis=1)
        x = jnp.concatenate([top, low], axis=0)
        rawx[j] = x
        squares += x * x
        lift[:, j * size : (j + 1) * size] = (x * mix_gain[j : j + 1, :]).astype(bf16)
    scale_in = lax.rsqrt(jnp.sum(squares, axis=1, keepdims=True) / depth + epsilon)
    total = rows_dot(lift[...], wproj[...]) * scale_in

    offset = lax.rem(z * width, size)
    scr_a[...] = jnp.zeros_like(scr_a)
    for x in range(4):
        piece = total[:, x * size : (x + 1) * size]
        if x < 2:
            scr_t[x] = piece
        scr_a[pl.ds(x, chips, stride=8), :] = pltpu.roll(
            piece.astype(bf16).astype(f32), offset, axis=1
        )
    send2[...] = scr_a[...].reshape(chips, 8, size).astype(bf16)
    for d in far_first(chips):
        send(send2.at[chip_at(d)], buf2.at[z], 1, d, c)
    buf2[z] = send2[z]

    lane = lax.broadcasted_iota(jnp.int32, (heads, size), 1)
    head = lax.broadcasted_iota(jnp.int32, (heads, size), 0)
    chosen = lane == head + width

    def own_column(x):
        row = jnp.broadcast_to(scr_t[x, pl.ds(z, 1), :], (heads, size))
        return jnp.sum(jnp.where(chosen, row, 0.0), axis=1, keepdims=True)

    def as_column(row):
        diagonal = lane[:, :heads] == head[:, :heads]
        spread = jnp.where(diagonal, jnp.broadcast_to(row, (heads, heads)), 0.0)
        return jnp.sum(spread, axis=1, keepdims=True)

    strength = jax.nn.sigmoid(own_column(0))
    rate_col = as_column(rate[...])
    bias_col = as_column(bias[...])
    lifted = own_column(1) + bias_col
    softplus = jnp.maximum(lifted, 0.0) + jnp.log(1.0 + jnp.exp(-jnp.abs(lifted)))
    retain = jnp.exp(-rate_col * softplus)
    state_copy.wait()

    arrived(buf2, chips - 1, 1)
    lane8 = lax.broadcasted_iota(jnp.int32, (8, size), 1)
    for h in range(heads):
        first = (h * size) // width
        tile = buf2[first].astype(f32)
        end = (first + 1) * width - h * size
        nxt = buf2[first + 1].astype(f32)
        scr_b[8 * h : 8 * h + 8, :] = jnp.where(lane8 < end, tile, nxt)
    query = scr_b[pl.ds(0, heads, stride=8), :]
    key = scr_b[pl.ds(1, heads, stride=8), :]
    value = scr_b[pl.ds(2, heads, stride=8), :]
    gate = scr_b[pl.ds(3, heads, stride=8), :]
    unit = key * lax.rsqrt(jnp.sum(key * key, axis=1, keepdims=True) + epsilon)

    def columns(rows):
        pad = jnp.zeros((16 - heads, size), f32)
        return jnp.concatenate([rows, pad], axis=0).T

    unit_cols = columns(unit)
    query_cols = columns(query)
    recall, asked = [], []
    for h in range(heads):
        s = state[h]
        recall.append(jnp.sum(s * unit_cols[:, h : h + 1], axis=0, keepdims=True))
        asked.append(jnp.sum(s * query_cols[:, h : h + 1], axis=0, keepdims=True))
    recall = jnp.concatenate(recall, axis=0)
    asked = jnp.concatenate(asked, axis=0)
    write = strength * (value - retain * recall)
    readout = retain * asked + jnp.sum(unit * query, axis=1, keepdims=True) * write
    normed = readout * lax.rsqrt(jnp.mean(readout * readout, axis=1, keepdims=True) + epsilon)
    normed = normed * head_gain[...] * (gate * jax.nn.sigmoid(gate))

    send3[0] = jnp.concatenate([normed, jnp.zeros((16 - heads, size), f32)], axis=0).astype(bf16)
    for d in far_first(chips):
        send(send3.at[0], buf3.at[z], 2, d, c)
    buf3[z] = send3[0]

    for h in range(heads):
        state_out[h] = (
            retain[h : h + 1, :] * state[h] + unit_cols[:, h : h + 1] * write[h : h + 1, :]
        )
    store_copy = pltpu.make_async_copy(state_out, new_memory_hbm, load_sem.at[9])
    store_copy.start()

    arrived(buf3, chips - 1, 2)
    for j in range(chips):
        scr_c[16 * j : 16 * j + 16, :] = buf3[j].astype(f32)
    mixed = jnp.concatenate(
        [scr_c[pl.ds(h, chips, stride=16), :].astype(bf16) for h in range(heads)], axis=1
    )
    branch = rows_dot(mixed, wout[...])
    middle = (rawx[z] + branch).astype(bf16)

    send4[0] = middle
    for d in far_first(chips):
        send(send4.at[0], buf4.at[z], 3, d, c)
    buf4[z] = middle
    middle_wide = middle.astype(f32)

    def split(tile):
        top, low = tile[:half_rows], tile[half_rows:]
        return (
            jnp.concatenate([top[:, :cols], low[:, :cols]], axis=1),
            jnp.concatenate([top[:, cols:], low[:, cols:]], axis=1),
        )

    for k, part in enumerate(split(middle_wide)):
        send4[1, 8 * k : 8 * k + 8] = part.astype(bf16)
        scr_o[8 * k : 8 * k + 8, :] = part
    mid_send = pltpu.make_async_remote_copy(
        src_ref=send4.at[1], dst_ref=midx, send_sem=send_sem.at[5], recv_sem=recv_sem.at[5],
        device_id={"kv": z, "tp": other}, device_id_type=MESH,
    )
    mid_send.start()
    for i in (5, 6):
        own_weights[i].wait()
        swap[i].wait_recv()
    mid_send.wait_recv()

    arrived(buf4, chips - 1, 3)
    squares = jnp.zeros((chips, size), f32)
    for j in range(chips):
        x = buf4[j].astype(f32)
        squares += x * x
        lift[:, j * size : (j + 1) * size] = (x * ffn_gain[j : j + 1, :]).astype(bf16)
    scale_mid = lax.rsqrt(jnp.sum(squares, axis=1, keepdims=True) / depth + epsilon)
    terms = None
    for k in range(2):
        raised = jnp.dot(lift[...], wup[k], preferred_element_type=f32)
        hidden = jnp.square(jnp.maximum(raised * scale_mid, 0.0)).astype(bf16)
        term = jnp.dot(hidden, wdown[k], preferred_element_type=f32)
        terms = term if terms is None else terms + term

    for j in range(chips):
        for k, part in enumerate(split(terms[:, j * size : (j + 1) * size])):
            send5[2 * j + k] = part.astype(bf16)
    for d in far_first(chips):
        for k in range(2):
            core = lax.rem(c + k, cores)
            send(send5.at[chip_at(d) * cores + core], buf5.at[me], 4, d, core)
    send(send5.at[z * cores + other], buf5.at[me], 4, 0, other)
    buf5[me] = send5[me]
    arrived(buf5, 2 * chips - 1, 4)
    mine = scr_o[pl.ds(pl.multiple_of(c * 8, 8), 8), :]
    halves = midx[...].astype(f32)
    theirs = jnp.where(c == 0, halves[0:8], halves[8:16])
    for k in range(2):
        down = buf5[k].astype(f32)
        for j in range(1, chips):
            down += buf5[2 * j + k].astype(f32)
        down += jnp.where(c == k, mine, theirs)
        tokf[pl.ds(k, half_rows, stride=2), :] = down
        tokf[pl.ds(chips + k, half_rows, stride=2), 0:cols] = down[:, cols:]
    out_ref[...] = tokf[:, 0:cols].astype(bf16)

    sent(buf1, 2 * chips - 1, 0)
    sent(buf2, chips - 1, 1)
    sent(buf3, chips - 1, 2)
    sent(buf4, chips - 1, 3)
    sent(buf5, 2 * chips - 1, 4)
    mid_send.wait_send()
    for copy in swap:
        copy.wait_send()
    store_copy.wait()


def per_device(
    tokens, memory, mix_gain, w_query, w_key, w_value, w_gate, w_beta, w_decay,
    decay_rate, decay_bias, head_gain, w_out, ffn_gain, w_up, w_down,
):
    chips = lax.axis_size("kv")
    rows, columns = tokens.shape
    depth = w_query.shape[0]
    heads = memory.shape[1]
    size = head_gain.shape[0]

    hbm = pl.BlockSpec(memory_space=pl.ANY)
    V = pltpu.VMEM
    DMA = pltpu.SemaphoreType.DMA
    state_shape = (heads, size, size)
    layer_out, new_memory = pl.pallas_call(
        layer_kernel,
        out_shape=(
            jax.ShapeDtypeStruct((rows, columns), bf16),
            jax.ShapeDtypeStruct(state_shape, f32),
        ),
        in_specs=[hbm] * 16,
        out_specs=(pl.BlockSpec(memory_space=pltpu.VMEM), hbm),
        scratch_shapes=[
            V((4 * size, depth), bf16), V((2, heads, depth), bf16),
            V((2 * columns, w_out.shape[0]), bf16), V((2,) + w_up.shape, bf16),
            V((2,) + w_down.shape, bf16),
            V(state_shape, f32), V(state_shape, f32), V(tokens.shape, bf16),
            V((depth // size, size), f32), V((depth // size, size), f32),
            V((1, heads), f32), V((1, heads), f32), V((1, size), f32),
            V((2, 8, size), bf16), V((2 * chips, 8, size), bf16),
            V((chips, 8, size), bf16), V((chips, 8, size), bf16),
            V((1, 16, size), bf16), V((chips, 16, size), bf16),
            V((2, 16, size), bf16), V((chips, 16, size), bf16),
            V((2 * chips, 8, size), bf16), V((2 * chips, 8, size), bf16),
            V((16, size), bf16),
            V((rows, size), f32), V((chips, chips, size), f32), V((chips, depth), bf16),
            V((2, chips, size), f32), V((chips * 8, size), f32), V((heads * 8, size), f32),
            V((chips * 16, size), f32), V((16, size), f32),
            DMA((10,)), DMA((7,)), DMA((7,)), DMA((7,)), DMA((6,)), DMA((6,)),
        ],
        compiler_params=pltpu.CompilerParams(collective_id=0, has_side_effects=True),
    )(
        tokens, memory.reshape(state_shape), mix_gain.reshape(-1, size), w_query.T, w_key.T,
        w_value.T, w_gate.T, w_beta.T, w_decay.T, decay_rate.reshape(1, heads),
        decay_bias.reshape(1, heads), head_gain.reshape(1, size), w_out.T,
        ffn_gain.reshape(-1, size), w_up, w_down,
    )
    return layer_out, new_memory.reshape(memory.shape)


def solution(mesh):
    lanes = ("kv", "tp")
    placed = (
        P(("grp", "dp"), lanes), P(("grp", "dp") + lanes, None, None), P(),
        P(None, lanes), P(None, lanes), P(None, lanes), P(None, lanes),
        P(), P(), P(), P(), P(), P(None, lanes), P(), P(None, lanes), P(lanes, None),
    )
    return jax.shard_map(
        per_device, mesh=mesh, in_specs=placed,
        out_specs=(P(("grp", "dp"), lanes), P(("grp", "dp") + lanes, None, None)),
        check_vma=False,
    )
```

time: 202 us -> 90.1 us (0.45)
  Pallas kernels: 0 us -> 85.9 us
  starting transfers between devices: 64.1 us -> 0 us
  waiting for transfers between devices: 58.8 us -> 0 us
  blocking collectives: 57.8 us -> 0 us
  local copies, waits for them, and re-layouts: 12.5 us -> 3.36 us
  matrix products: 3.54 us -> 0 us
  other arithmetic: 3.47 us -> 0 us
    pallas_call x0 -> x1, Pallas kernels: none -> 85.9 us  [per_device(): pl.pallas_call(layer_kernel, out_shape=(jax.ShapeDtypeStruct((rows, colum...]
    all_to_all x5 -> x0, starting transfers between devices: 64.1 us -> none  [the longest x1 45.2 us: from_everyone(): lax.all_to_all(jnp.broadcast_to(value[None], (size, *value.shape)), axis,...]
    all_to_all x5 -> x0, waiting for transfers between devices: 58.8 us -> none  [the longest x4 42.8 us: per_device(): lax.all_to_all(shortened(sent), ('kv', 'tp'), split_axis=0, concat_axis=1...]
    all_to_all x4 -> x0, blocking collectives: 57.8 us -> none  [the longest x2 38.5 us: from_everyone(): lax.all_to_all(jnp.broadcast_to(value[None], (size, *value.shape)), axis,...]
    dot_general x10 -> x0, matrix products: 3.54 us -> none  [the longest x2 1.58 us: fold_proj(): jnp.dot(mine, weight, preferred_element_type=jnp.float32)]
    unnamed x44 -> x2, local copies, waits for them, and re-layouts: 6.18 us -> 3.36 us
    all_to_all x4 -> x0, local copies, waits for them, and re-layouts: 2.56 us -> none  [per_device(): lax.all_to_all(shortened(sent), ('kv', 'tp'), split_axis=0, concat_axis=1...]
  transfers between devices with their start and end apart: 5 -> 0, of which waited for: 5 -> 0; matrix products, arithmetic and copies ran while one was open for 2% -> 0% of each run, Pallas kernels for 0% -> 0%
where the time goes in v1:
time: 90.1 us; the launch traced here: 89.9 us
  Pallas kernels  85.9 us (95%)
  local copies, waits for them, and re-layouts  3.36 us (4%)
    pallas_call x1, Pallas kernels, per_device(): pl.pallas_call(layer_kernel, out_shape=(jax.ShapeDtypeStruct((rows, colum...  85.9 us
    unnamed x2, local copies, waits for them, and re-layouts  3.36 us

profile of v1, /device:TPU:65, one launch (start us, length us, event | category | flops | bytes accessed | tf_op | source)
XLA Modules:
  0.0 89.9 jit_solution(2476323065019188258)
XLA Ops:
  0.6 85.9 %shard_map.167 = (bf16[32,64]{1,0:T(8,128)(2,1)}, f32[12,128,128]{2,1,0:T(8,128)}) custom-call(bf16[32,64]{1,0:T(8,128)(2,1)} %tokens_hbm.1, f32[12,128,128]{2,1,0:T(8,128)} %bitcast.15, f32[16,128]{1,0:T(8,128)} %bitcast.23, bf16[48,2048]{1,0:T(8,128)(2,1)} %bitcast.16, bf16[48,2048]{1,0:T(8,128)(2,1)} %bitcast.17, bf16[48,2048]{1,0:T(8,128)(2,1)} %bitcast.18, ...), custom_call_target="tpu_custom_call" | custom-call | tf_op jit(solution)/shard_map/pallas_call | solution.py:335
  86.5 1.3 %copy.22 = bf16[32,64]{1,0:T(8,128)(2,1)} copy(bf16[32,64]{1,0:T(8,128)(2,1)} %get-tuple-element.12) | data formatting | bytes 8192
  87.8 2.1 %copy.23 = f32[1,12,16384]{2,0,1:T(1,128)} copy(f32[1,12,16384]{2,0,1:T(1,128)} %bitcast.14) | data formatting | bytes 1572864
